TPU v7x, 512 devices: a whole 4x8x8 slice. The times are simulated.
512 devices in a mesh: sp: 32 (over z, x), tp: 16 (over y, core).
Axes of the slice: x: 4, y: 8, z: 8, core: 2. Of those that a mesh axis runs over, the one named last changes fastest.
Arguments:
- queries: bfloat16 [8192, 2048], P('sp', 'tp'), may hold values from -6 to 6
- keys: bfloat16 [8192, 1024], P('sp', 'tp'), may hold values from -6 to 6
- values: bfloat16 [8192, 1024], P('sp', 'tp'), may hold values from -6 to 6
- docs: int32 [8192], P('sp'), may hold values from 0 to 2, never falling along the last dimension, each value on 1 to 5120 neighbouring positions
- query_gain: float32 [64], replicated, may hold values from 0.5 to 8
- key_gain: float32 [64], replicated, may hold values from 0.5 to 8
- out_weight: bfloat16 [2048, 2048], P('tp'), may hold values from -0.125 to 0.125
- residual: bfloat16 [8192, 2048], P('sp', 'tp'), may hold values from -12 to 12
- norm_gain: float32 [2048], P('tp'), may hold values from 0.1 to 1.9
- routes: int32 [8192, 2], P('sp'), may hold values from 0 to 31, all different within a row; in each aligned block of 256 rows (0 to 255, 256 to 511, ...) at most 20 rows name the same one
- route_weight: float32 [8192, 2], P('sp'), may hold values from 0.1 to 1
- gate_weight: bfloat16 [32, 2048, 4096], P('sp', None, 'tp'), may hold values from -0.3125 to 0.3125
- up_weight: bfloat16 [32, 2048, 4096], P('sp', None, 'tp'), may hold values from -0.3125 to 0.3125
- down_weight: bfloat16 [32, 4096, 2048], P('sp', 'tp'), may hold values from -0.09375 to 0.09375
Outputs:
- mixed: bfloat16 [8192, 2048], P('sp', 'tp')
Inputs may be any that keep to these rules, and one draw needn't show every extreme that they name: `routes`: in each aligned block of 256 rows no expert is named by more than 20 rows, and 20 is reached in some block; a row names 2 different experts. `docs`: document numbers never fall along the sequence; a document holds at most 5120 positions.
All inputs are finite; a program needn't handle non-finite values.
Results may differ from a plain program's by a relative error of at most 0.028.
The roundings to bfloat16 on the way count: a program that leaves them out, or rounds other values in their place, can miss the bound.
Values may be sent and summed in bfloat16 or wider, within the bound.
No kernel may reach another device: no remote copies, remote signals or barrier semaphores. Data moves between devices by JAX's collectives and lax.ppermute only.
A program may use at most 64 MiB of HBM per device.

v0:
```python
import jax
import jax.numpy as jnp
from jax import lax
from jax.sharding import PartitionSpec as P

GRID_W = 64
EPSILON = 1e-06
NEG_BIG = -1e30
ROTARY_BASE = 10000.0
CLAMP_LIMIT = 7.0
SIGMOID_SCALE = 1.702


def sent_together(arrays, axis, dim, along):
    columns = [a.reshape(*a.shape[:along], -1) for a in arrays]
    both = jnp.concatenate(columns, axis=along)
    out, at, gathered = (lax.all_gather(both, axis, axis=dim, tiled=True), 0, [])
    for a, column in zip(arrays, columns):
        piece = out[..., at : at + column.shape[along]]
        gathered.append(piece.reshape(*piece.shape[:along], *a.shape[along:]))
        at += column.shape[along]
    return tuple(gathered)


def cut_along(value, dim, length):
    before, after = (value.shape[:dim], value.shape[dim + 1 :])
    return jnp.moveaxis(value.reshape(*before, length, -1, *after), dim, 0)


def summed_on_arrival(value, axis, dim):
    length = lax.axis_size(axis)
    tiles = lax.all_to_all(cut_along(value, dim, length), axis, 0, 0, tiled=True)
    return jnp.sum(tiles.astype(jnp.float32), axis=0)


def copy_for_each(value, axis):
    length = lax.axis_size(axis)
    return lax.all_to_all(
        jnp.broadcast_to(value[None], (length, *value.shape)), axis, 0, 0, tiled=True
    )


def of_everyone(value, axis):
    everything = copy_for_each(value, axis)
    return jnp.sum(everything, axis=0)


def rope_tables(positions, head_dim):
    quarter = head_dim // 4
    freqs = ROTARY_BASE ** (-jnp.arange(quarter, dtype=jnp.float32) / quarter)
    row_pos = (positions // GRID_W).astype(jnp.float32)
    col_pos = (positions % GRID_W).astype(jnp.float32)
    angle = jnp.concatenate([row_pos[:, None] * freqs, col_pos[:, None] * freqs], axis=1)
    return (jnp.cos(angle), jnp.sin(angle))


def norm_rotate(heads, gain, cosine_table, sine_table):
    entries = heads.astype(jnp.float32)
    entries = (
        entries * lax.rsqrt(jnp.mean(entries * entries, axis=-1, keepdims=True) + EPSILON) * gain
    )
    pairs = entries.reshape(entries.shape[:-1] + (entries.shape[-1] // 2, 2))
    first = pairs[..., 0]
    second = pairs[..., 1]
    cos_rows = cosine_table[:, None, :]
    sin_rows = sine_table[:, None, :]
    turned = jnp.stack(
        [first * cos_rows - second * sin_rows, first * sin_rows + second * cos_rows], axis=-1
    )
    return turned.reshape(heads.shape).astype(jnp.bfloat16)


def clamped_unit(gate_pre, up_pre):
    bounded = jnp.minimum(gate_pre, CLAMP_LIMIT)
    linear = jnp.clip(up_pre, -CLAMP_LIMIT, CLAMP_LIMIT)
    return (bounded * jax.nn.sigmoid(SIGMOID_SCALE * bounded) * (linear + 1.0)).astype(jnp.bfloat16)


def block_length(length):
    block_size = length
    while block_size > 2048 and block_size % 2 == 0:
        block_size = block_size // 2
    return block_size


def softmax_update(running, inputs, query_rot, own_tags, score_scale):
    row_peak, denominator, carried = running
    key_block, value_block, tag_block = inputs
    scores = (
        jnp.einsum("tkgd,pkd->tkgp", query_rot, key_block, preferred_element_type=jnp.float32)
        * score_scale
    )
    allowed = own_tags[:, None, None, None] == tag_block[None, None, None, :]
    scores = jnp.where(allowed, scores, NEG_BIG)
    new_peak = jnp.maximum(row_peak, jnp.max(scores, axis=-1))
    weights = jnp.where(allowed, jnp.exp(scores - new_peak[..., None]), 0.0)
    factor = jnp.exp(row_peak - new_peak)
    denominator = denominator * factor + jnp.sum(weights, axis=-1)
    carried = carried * factor[..., None] + jnp.einsum(
        "tkgp,pkd->tkgd",
        weights.astype(jnp.bfloat16),
        value_block,
        preferred_element_type=jnp.float32,
    )
    return (new_peak, denominator, carried)


def per_device(
    queries,
    keys,
    values,
    docs,
    query_gain,
    key_gain,
    out_weight,
    residual,
    norm_gain,
    routes,
    route_weight,
    gate_weight,
    up_weight,
    down_weight,
):
    tokens = queries.shape[0]
    head_dim = query_gain.shape[0]
    query_heads = queries.shape[1] // head_dim
    pair_heads = keys.shape[1] // head_dim
    pair_width = keys.shape[1]
    positions = lax.axis_index("sp") * tokens + jnp.arange(tokens, dtype=jnp.int32)
    cosine_table, sine_table = rope_tables(positions, head_dim)
    query_rot = norm_rotate(
        queries.reshape(tokens, query_heads, head_dim), query_gain, cosine_table, sine_table
    )
    query_rot = query_rot.reshape(tokens, pair_heads, 2, head_dim)
    key_rot = norm_rotate(
        keys.reshape(tokens, pair_heads, head_dim), key_gain, cosine_table, sine_table
    )
    stacked = jnp.concatenate([key_rot.reshape(tokens, pair_width), values], axis=1)
    own_tags = docs.astype(jnp.bfloat16)
    score_scale = head_dim ** (-0.5)
    stat_shape = (tokens, pair_heads, 2)
    initial = (
        jnp.full(stat_shape, NEG_BIG, jnp.float32),
        jnp.zeros(stat_shape, jnp.float32),
        jnp.zeros(stat_shape + (head_dim,), jnp.float32),
    )
    pair_rows, tag_rows = sent_together((stacked, own_tags), "sp", 0, 1)
    length = pair_rows.shape[0]
    block_size = block_length(length)
    blocks = length // block_size
    key_part = pair_rows[:, :pair_width].reshape(blocks, block_size, pair_heads, head_dim)
    value_part = pair_rows[:, pair_width:].reshape(blocks, block_size, pair_heads, head_dim)
    tag_part = tag_rows.reshape(blocks, block_size)

    def advance(carry_state, inputs):
        return (softmax_update(carry_state, inputs, query_rot, own_tags, score_scale), None)

    result, _ = lax.scan(advance, initial, (key_part, value_part, tag_part))
    row_peak, denominator, carried = result
    attended = (
        (carried / denominator[..., None])
        .astype(jnp.bfloat16)
        .reshape(tokens, query_heads * head_dim)
    )
    width_local = residual.shape[1]
    projected = summed_on_arrival(
        lax.dot_general(
            out_weight, attended, (((0,), (1,)), ((), ())), preferred_element_type=jnp.float32
        ).astype(jnp.bfloat16),
        "tp",
        0,
    )
    mixed_first = residual.astype(jnp.float32) + projected.T
    squares = of_everyone(jnp.sum(mixed_first * mixed_first, axis=1), "tp")
    full_width = width_local * lax.axis_size("tp")
    normed = (mixed_first * lax.rsqrt(squares / full_width + EPSILON)[:, None] * norm_gain).astype(
        jnp.bfloat16
    )
    experts = lax.axis_size("sp")
    top_count = routes.shape[1]
    capacity = max(2, 5 * tokens * top_count // (4 * experts))
    flat_routes = routes.reshape(-1)
    entries = flat_routes.shape[0]
    expert_ids = jnp.arange(experts, dtype=jnp.int32)
    onehot = (flat_routes[:, None] == expert_ids[None, :]).astype(jnp.int32)
    earlier = jnp.cumsum(onehot, axis=0) - onehot
    slot_index = jnp.sum(earlier * onehot, axis=1)
    slot_ids = jnp.arange(capacity, dtype=jnp.int32)
    matches = (flat_routes[:, None, None] == expert_ids[None, :, None]) & (
        slot_index[:, None, None] == slot_ids[None, None, :]
    )
    entry_ids = jnp.arange(entries, dtype=jnp.int32)
    source_entry = jnp.sum(jnp.where(matches, entry_ids[:, None, None], 0), axis=0)
    occupied = jnp.any(matches, axis=0)
    source_row = source_entry // top_count
    gate_local = gate_weight[0]
    up_local = up_weight[0]
    down_local = down_weight[0]
    model_width = gate_local.shape[0]
    outgoing = jnp.where(occupied[..., None], normed[source_row], jnp.zeros((), jnp.bfloat16))
    arrived = lax.all_to_all(outgoing, "sp", split_axis=0, concat_axis=0, tiled=True)
    sources = arrived.shape[0]
    flat_rows = arrived.reshape(-1, width_local)
    column_piece = lax.all_gather(flat_rows, "tp", axis=1, tiled=True)
    gate_pre = jnp.dot(column_piece, gate_local, preferred_element_type=jnp.float32)
    up_pre = jnp.dot(column_piece, up_local, preferred_element_type=jnp.float32)
    hidden = clamped_unit(gate_pre, up_pre)
    partial_value = jnp.dot(hidden, down_local, preferred_element_type=jnp.float32).reshape(
        sources, capacity, model_width
    )
    expert_out = summed_on_arrival(partial_value.astype(jnp.bfloat16), "tp", 2).astype(jnp.bfloat16)
    returned = lax.all_to_all(expert_out, "sp", split_axis=0, concat_axis=0, tiled=True)
    lookup = flat_routes * capacity + slot_index
    picked = (
        returned.reshape(-1, width_local)[lookup]
        .reshape(tokens, top_count, width_local)
        .astype(jnp.float32)
    )
    routed = jnp.sum(route_weight[:, :, None] * picked, axis=1)
    return (mixed_first + routed).astype(jnp.bfloat16)


def solution(mesh):
    in_specs = (
        P("sp", "tp"),
        P("sp", "tp"),
        P("sp", "tp"),
        P("sp"),
        P(),
        P(),
        P("tp", None),
        P("sp", "tp"),
        P("tp"),
        P("sp", None),
        P("sp", None),
        P("sp", None, "tp"),
        P("sp", None, "tp"),
        P("sp", "tp", None),
    )
    out_specs = P("sp", "tp")
    return jax.shard_map(
        per_device, mesh=mesh, in_specs=in_specs, out_specs=out_specs, check_vma=False
    )
```

profile of v0, /device:TPU:24, one launch (start us, length us, event | category | flops | bytes accessed | tf_op | source)
XLA Modules:
  0.0 353.9 jit_solution(10780892546366876018)
XLA Ops:
  13.3 83.1 %all-gather.3.cloned.1.call-done = bf16[8192,129]{0,1:T(8,128)(2,1)} async-done(((bf16[256,129]{0,1:T(8,128)(2,1)}), bf16[8192,129]{0,1:T(8,128)(2,1)}) %all-gather.3.cloned.1.call-update) | async-done | bytes 2113552 | tf_op jit(solution)/shard_map/all_gather | solution.py:17
  96.4 2.7 fusion.54
  105.9 35.0 %while.15 = (s32[]{:T(128)}, f32[256,1,2]{0,2,1:T(2,128)S(1)}, f32[256,1,2]{0,2,1:T(2,128)S(1)}, f32[256,1,2,64]{0,3,2,1:T(8,128)S(1)}, bf16[256]{0:T(256)(128)(...) while((s32[]{:T(128)}, f32[256,1,2]{0,2,1:T(2,128)S(1)}, ...), condition=%wide.region_5.6_spmd.clone, body=%wide.region_2.5_spmd.clone.sunk | while | flops 282692608 | bytes 32355992 | solution.py:158
  106.3 3.6 %fusion.68 = (f32[256,2]{0,1:T(2,128)S(1)}, f32[2048,256,2]{1,0,2:T(8,128)}) fusion(pred[256,2048]{0,1:T(8,128)(4,1)S(1)} %broadcast_compare_fusion.3, bf16[256,1,2,64]{0,3,2,1:T(8,128)(2,1)S(1)} %get-tuple-element.262, bf16[4,2048,1,64]{1,3,2,0:T(8,128)(2,1)} %get-tuple-element.261, s32[]{:T(128)} %get-tuple-element.244), kind=kOutput, calls=%fused_computation.4.clone.1 | convolution fusion | flops 137362944 | bytes 5048832 | tf_op jit(solution)/shard_map/while/body/eval_jaxpr/tkgd,pkd->tkgp/dot_general | solution.py:90
  110.0 3.5 fusion.71
  115.1 3.6 %fusion.68 = (f32[256,2]{0,1:T(2,128)S(1)}, f32[2048,256,2]{1,0,2:T(8,128)}) fusion(pred[256,2048]{0,1:T(8,128)(4,1)S(1)} %broadcast_compare_fusion.3, bf16[256,1,2,64]{0,3,2,1:T(8,128)(2,1)S(1)} %get-tuple-element.262, bf16[4,2048,1,64]{1,3,2,0:T(8,128)(2,1)} %get-tuple-element.261, s32[]{:T(128)} %get-tuple-element.244), kind=kOutput, calls=%fused_computation.4.clone.1 | convolution fusion | flops 137362944 | bytes 5048832 | tf_op jit(solution)/shard_map/while/body/eval_jaxpr/tkgd,pkd->tkgp/dot_general | solution.py:90
  118.7 3.5 fusion.71
  123.8 3.6 %fusion.68 = (f32[256,2]{0,1:T(2,128)S(1)}, f32[2048,256,2]{1,0,2:T(8,128)}) fusion(pred[256,2048]{0,1:T(8,128)(4,1)S(1)} %broadcast_compare_fusion.3, bf16[256,1,2,64]{0,3,2,1:T(8,128)(2,1)S(1)} %get-tuple-element.262, bf16[4,2048,1,64]{1,3,2,0:T(8,128)(2,1)} %get-tuple-element.261, s32[]{:T(128)} %get-tuple-element.244), kind=kOutput, calls=%fused_computation.4.clone.1 | convolution fusion | flops 137362944 | bytes 5048832 | tf_op jit(solution)/shard_map/while/body/eval_jaxpr/tkgd,pkd->tkgp/dot_general | solution.py:90
  127.5 3.5 fusion.71
  132.6 3.6 %fusion.68 = (f32[256,2]{0,1:T(2,128)S(1)}, f32[2048,256,2]{1,0,2:T(8,128)}) fusion(pred[256,2048]{0,1:T(8,128)(4,1)S(1)} %broadcast_compare_fusion.3, bf16[256,1,2,64]{0,3,2,1:T(8,128)(2,1)S(1)} %get-tuple-element.262, bf16[4,2048,1,64]{1,3,2,0:T(8,128)(2,1)} %get-tuple-element.261, s32[]{:T(128)} %get-tuple-element.244), kind=kOutput, calls=%fused_computation.4.clone.1 | convolution fusion | flops 137362944 | bytes 5048832 | tf_op jit(solution)/shard_map/while/body/eval_jaxpr/tkgd,pkd->tkgp/dot_general | solution.py:90
  136.2 3.5 fusion.71
  142.7 7.4 %all-to-all-start = ((bf16[16,128,256]{1,2,0:T(8,128)(2,1)}), bf16[16,128,256]{1,2,0:T(8,128)(2,1)S(1)}, u32[]{:S(2)}, u32[]{:S(2)}) async-start(bf16[16,128,256]{1,2,0:T(8,128)(2,1)} %bitcast.153), calls=%async_computation | async-start | bytes 2097152 | tf_op jit(solution)/shard_map/all_to_all | solution.py:32
  153.2 23.1 %all-to-all-done = bf16[16,128,256]{1,2,0:T(8,128)(2,1)S(1)} async-done(((bf16[16,128,256]{1,2,0:T(8,128)(2,1)}), bf16[16,128,256]{1,2,0:T(8,128)(2,1)S(1)}, u32[]{:S(2)}, u32[]{:S(2)}) %all-to-all-start) | async-done | bytes 1048608 | tf_op jit(solution)/shard_map/all_to_all | solution.py:32
  177.2 5.2 %all-to-all-start.1 = ((f32[16,1,256]{2,1,0:T(1,128)}), f32[16,1,256]{2,1,0:T(1,128)S(1)}, u32[]{:S(2)}, u32[]{:S(2)}) async-start(f32[16,1,256]{2,1,0:T(1,128)} %broadcast_in_dim.54), calls=%async_computation.1 | async-start | bytes 32768 | tf_op jit(solution)/shard_map/all_to_all | solution.py:38
  182.5 4.4 %all-to-all-done.1 = f32[16,1,256]{2,1,0:T(1,128)S(1)} async-done(((f32[16,1,256]{2,1,0:T(1,128)}), f32[16,1,256]{2,1,0:T(1,128)S(1)}, u32[]{:S(2)}, u32[]{:S(2)}) %all-to-all-start.1) | async-done | bytes 16416 | tf_op jit(solution)/shard_map/all_to_all | solution.py:38
  189.3 19.4 %all_to_all.26 = bf16[32,20,128]{2,1,0:T(8,128)(2,1)S(1)} all-to-all(bf16[32,20,128]{2,1,0:T(8,128)(2,1)S(1)} %broadcast_select_fusion.1), channel_id=1, replica_groups=mesh['sp'=32,'tp'=16] {'sp'}, dimensions={0} | all-to-all | bytes 327680 | tf_op jit(solution)/shard_map/all_to_all | solution.py:201
  209.4 37.6 %all-gather.5.cloned.1.call-done = bf16[640,2048]{1,0:T(8,128)(2,1)} async-done(((bf16[640,128]{1,0:T(8,128)(2,1)}), bf16[640,2048]{1,0:T(8,128)(2,1)}) %all-gather.5.cloned.1.call-update) | async-done | bytes 2621456 | tf_op jit(solution)/shard_map/all_gather | solution.py:204
  247.1 2.7 convolution_minimum_fusion
  251.7 2.2 copy.126
  253.9 5.8 %all-to-all-start.3 = ((bf16[16,32,20,128]{3,1,2,0:T(8,128)(2,1)}), bf16[16,32,20,128]{3,1,2,0:T(8,128)(2,1)}, u32[]{:S(2)}, u32[]{:S(2)}) async-start(bf16[16,32,20,128]{3,1,2,0:T(8,128)(2,1)} %bitcast.176), calls=%async_computation.3 | async-start | bytes 5242880 | tf_op jit(solution)/shard_map/all_to_all | solution.py:32
  260.1 59.6 %all-to-all-done.3 = bf16[16,32,20,128]{3,1,2,0:T(8,128)(2,1)} async-done(((bf16[16,32,20,128]{3,1,2,0:T(8,128)(2,1)}), bf16[16,32,20,128]{3,1,2,0:T(8,128)(2,1)}, u32[]{:S(2)}, u32[]{:S(2)}) %all-to-all-start.3) | async-done | bytes 2621472 | tf_op jit(solution)/shard_map/all_to_all | solution.py:32
  319.7 2.1 reduce_sum.107
  322.6 10.2 %all-to-all-start.4 = ((bf16[32,20,128]{2,1,0:T(8,128)(2,1)}), bf16[32,20,128]{2,1,0:T(8,128)(2,1)S(1)}, u32[]{:S(2)}, u32[]{:S(2)}) async-start(bf16[32,20,128]{2,1,0:T(8,128)(2,1)} %copy.107), calls=%async_computation.4 | async-start | bytes 393216 | tf_op jit(solution)/shard_map/all_to_all | solution.py:212
  332.8 11.8 %all-to-all-done.4 = bf16[32,20,128]{2,1,0:T(8,128)(2,1)S(1)} async-done(((bf16[32,20,128]{2,1,0:T(8,128)(2,1)}), bf16[32,20,128]{2,1,0:T(8,128)(2,1)S(1)}, u32[]{:S(2)}, u32[]{:S(2)}) %all-to-all-start.4) | async-done | bytes 163872 | tf_op jit(solution)/shard_map/all_to_all | solution.py:212
  (133 shorter events, 34.1 us)
Async XLA Ops:
  6.5 244.3 %copy-start = (bf16[1,256,2048]{2,1,0:T(8,128)(2,1)S(1)}, bf16[1,256,2048]{2,1,0:T(8,128)(2,1)}, u32[]{:S(2)}) copy-start(bf16[1,256,2048]{2,1,0:T(8,128)(2,1)} %param.29) | copy-start | bytes 3145732
  6.5 89.9 %all-gather.3.cloned.1.call-start = ((), (), s32[]{:S(2)}) async-start(), calls=%async_computation.5 | async-start | bytes 2297856 | tf_op jit(solution)/shard_map/all_gather | solution.py:17
  105.9 35.1 %copy-start.3 = (bf16[128,2048]{1,0:T(8,128)(2,1)S(1)}, bf16[128,2048]{1,0:T(8,128)(2,1)}, u32[]{:S(2)}) copy-start(bf16[128,2048]{1,0:T(8,128)(2,1)} %param.22) | copy-start | bytes 1572868
  110.0 3.5 copy-start.1
  118.7 3.5 copy-start.1
  127.5 3.5 copy-start.1
  136.2 3.5 copy-start.1
  140.9 9.2 %copy-start.4 = (s32[256,2]{0,1:T(2,128)S(1)}, s32[256,2]{0,1:T(2,128)}, u32[]{:S(2)}) copy-start(s32[256,2]{0,1:T(2,128)} %param.25) | copy-start | bytes 6148
  140.9 35.5 %copy-start.2 = (bf16[256,128]{1,0:T(8,128)(2,1)S(1)}, bf16[256,128]{1,0:T(8,128)(2,1)}, u32[]{:S(2)}) copy-start(bf16[256,128]{1,0:T(8,128)(2,1)} %param.23) | copy-start | bytes 196612
  140.9 46.0 %copy-start.6 = (f32[128]{0:T(128)S(1)}, f32[128]{0:T(128)}, u32[]{:S(2)}) copy-start(f32[128]{0:T(128)} %param.24) | copy-start | bytes 1540
  142.7 104.4 %copy-start.8 = (bf16[1,2048,256]{2,1,0:T(8,128)(2,1)S(1)}, bf16[1,2048,256]{2,1,0:T(8,128)(2,1)}, u32[]{:S(2)}) copy-start(bf16[1,2048,256]{2,1,0:T(8,128)(2,1)} %param.27) | copy-start | bytes 3145732
  142.7 33.6 %all-to-all-start = ((bf16[16,128,256]{1,2,0:T(8,128)(2,1)}), bf16[16,128,256]{1,2,0:T(8,128)(2,1)S(1)}, u32[]{:S(2)}, u32[]{:S(2)}) async-start(bf16[16,128,256]{1,2,0:T(8,128)(2,1)} %bitcast.153), calls=%async_computation | async-start | bytes 2097152 | tf_op jit(solution)/shard_map/all_to_all | solution.py:32
  177.2 9.7 %all-to-all-start.1 = ((f32[16,1,256]{2,1,0:T(1,128)}), f32[16,1,256]{2,1,0:T(1,128)S(1)}, u32[]{:S(2)}, u32[]{:S(2)}) async-start(f32[16,1,256]{2,1,0:T(1,128)} %broadcast_in_dim.54), calls=%async_computation.1 | async-start | bytes 32768 | tf_op jit(solution)/shard_map/all_to_all | solution.py:38
  182.4 64.7 %all-gather.5.cloned.1.call-start = ((), (), s32[]{:S(2)}) async-start(), calls=%async_computation.6 | async-start | bytes 2785280 | tf_op jit(solution)/shard_map/all_gather | solution.py:204
  247.0 2.8 copy-start.7
  247.1 2.8 copy-start.9
  251.7 8.3 %copy-start.5 = (f32[256,2]{0,1:T(2,128)S(1)}, f32[256,2]{0,1:T(2,128)}, u32[]{:S(2)}) copy-start(f32[256,2]{0,1:T(2,128)} %param.26) | copy-start | bytes 6148
  253.9 65.8 %all-to-all-start.3 = ((bf16[16,32,20,128]{3,1,2,0:T(8,128)(2,1)}), bf16[16,32,20,128]{3,1,2,0:T(8,128)(2,1)}, u32[]{:S(2)}, u32[]{:S(2)}) async-start(bf16[16,32,20,128]{3,1,2,0:T(8,128)(2,1)} %bitcast.176), calls=%async_computation.3 | async-start | bytes 5242880 | tf_op jit(solution)/shard_map/all_to_all | solution.py:32
  322.6 22.1 %all-to-all-start.4 = ((bf16[32,20,128]{2,1,0:T(8,128)(2,1)}), bf16[32,20,128]{2,1,0:T(8,128)(2,1)S(1)}, u32[]{:S(2)}, u32[]{:S(2)}) async-start(bf16[32,20,128]{2,1,0:T(8,128)(2,1)} %copy.107), calls=%async_computation.4 | async-start | bytes 393216 | tf_op jit(solution)/shard_map/all_to_all | solution.py:212
Sparse Core Ops, SparseCore 0:
  10.9 85.4 all-gather.2
  209.6 37.4 all-gather.4
where the time goes:
time: 355 us; the launch traced here: 354 us
  waiting for transfers between devices  220 us (62%)
  matrix products  33.4 us (9%)
  starting transfers between devices  28.6 us (8%)
  local copies, waits for them, and re-layouts  22.1 us (6%)
  blocking collectives  19.4 us (5%)
  other arithmetic  16.7 us (5%)
  between operations  13.9 us (4%)
    all_gather x1, waiting for transfers between devices, sent_together(): lax.all_gather(both, axis, axis=dim, tiled=True)  83.1 us
    all_to_all x2, waiting for transfers between devices, summed_on_arrival(): lax.all_to_all(cut_along(value, dim, length), axis, 0, 0, tiled=True)  82.7 us
    all_gather x1, waiting for transfers between devices, per_device(): column_piece = lax.all_gather(flat_rows, 'tp', axis=1, tiled=True)  37.6 us
    all_to_all x1, blocking collectives, per_device(): lax.all_to_all(outgoing, 'sp', split_axis=0, concat_axis=0, tiled=True)  19.4 us
    dot_general x4, matrix products, softmax_update(): jnp.einsum('tkgd,pkd->tkgp', query_rot, key_block, preferred_element_type...  14.5 us
    dot_general x4, matrix products, softmax_update(): jnp.einsum('tkgp,pkd->tkgd', weights.astype(jnp.bfloat16), value_block, p...  13.9 us
    all_to_all x2, starting transfers between devices, summed_on_arrival(): lax.all_to_all(cut_along(value, dim, length), axis, 0, 0, tiled=True)  13.2 us
    all_to_all x1, waiting for transfers between devices, per_device(): lax.all_to_all(expert_out, 'sp', split_axis=0, concat_axis=0, tiled=True)  11.8 us
  transfers between devices with their start and end apart: 6, of which 6 were waited for; matrix products, arithmetic and copies ran while one was open for 2% of the time, Pallas kernels for 0%

commit v1 on v0

--- a/solution.py
+++ b/solution.py
@@ -201,7 +201,9 @@
     arrived = lax.all_to_all(outgoing, "sp", split_axis=0, concat_axis=0, tiled=True)
     sources = arrived.shape[0]
     flat_rows = arrived.reshape(-1, width_local)
-    column_piece = lax.all_gather(flat_rows, "tp", axis=1, tiled=True)
+    column_piece = jnp.concatenate(
+        lax.all_to_all(jnp.stack([flat_rows] * lax.axis_size("tp")), "tp", 0, 0), axis=1
+    )
     gate_pre = jnp.dot(column_piece, gate_local, preferred_element_type=jnp.float32)
     up_pre = jnp.dot(column_piece, up_local, preferred_element_type=jnp.float32)
     hidden = clamped_unit(gate_pre, up_pre)

time: 355 us -> 375 us (1.056)
  blocking collectives: 19.4 us -> 85.1 us
  waiting for transfers between devices: 220 us -> 183 us
  starting transfers between devices: 28.6 us -> 21.6 us
    all_to_all x0 -> x1, blocking collectives: none -> 65.6 us  [per_device(): lax.all_to_all(jnp.stack([flat_rows] * lax.axis_size('tp')), 'tp', 0, 0)]
    all_gather x1 -> x0, waiting for transfers between devices: 37.6 us -> none  [per_device(): column_piece = lax.all_gather(flat_rows, 'tp', axis=1, tiled=True)]
    all_to_all x1, starting transfers between devices: 10.2 us -> 3.86 us  [per_device(): lax.all_to_all(expert_out, 'sp', split_axis=0, concat_axis=0, tiled=True)]
  transfers between devices with their start and end apart: 6 -> 5, of which waited for: 6 -> 5; matrix products, arithmetic and copies ran while one was open for 2% -> 2% of each run, Pallas kernels for 0% -> 0%
where the time goes in v1:
time: 375 us; the launch traced here: 374 us
  waiting for transfers between devices  183 us (49%)
  blocking collectives  85.1 us (23%)
  matrix products  31.5 us (8%)
  local copies, waits for them, and re-layouts  22.2 us (6%)
  starting transfers between devices  21.6 us (6%)
  other arithmetic  16.7 us (4%)
  between operations  13.8 us (4%)
    all_gather x1, waiting for transfers between devices, sent_together(): lax.all_gather(both, axis, axis=dim, tiled=True)  83.1 us
    all_to_all x2, waiting for transfers between devices, summed_on_arrival(): lax.all_to_all(cut_along(value, dim, length), axis, 0, 0, tiled=True)  82.7 us
    all_to_all x1, blocking collectives, per_device(): lax.all_to_all(jnp.stack([flat_rows] * lax.axis_size('tp')), 'tp', 0, 0)  65.6 us
    all_to_all x1, blocking collectives, per_device(): lax.all_to_all(outgoing, 'sp', split_axis=0, concat_axis=0, tiled=True)  19.4 us
    dot_general x4, matrix products, softmax_update(): jnp.einsum('tkgd,pkd->tkgp', query_rot, key_block, preferred_element_type...  14.5 us
    dot_general x4, matrix products, softmax_update(): jnp.einsum('tkgp,pkd->tkgd', weights.astype(jnp.bfloat16), value_block, p...  13.9 us
    all_to_all x2, starting transfers between devices, summed_on_arrival(): lax.all_to_all(cut_along(value, dim, length), axis, 0, 0, tiled=True)  12.5 us
    all_to_all x1, waiting for transfers between devices, per_device(): lax.all_to_all(expert_out, 'sp', split_axis=0, concat_axis=0, tiled=True)  12.3 us
  transfers between devices with their start and end apart: 5, of which 5 were waited for; matrix products, arithmetic and copies ran while one was open for 2% of the time, Pallas kernels for 0%

profile of v1, /device:TPU:24, one launch (start us, length us, event | category | flops | bytes accessed | tf_op | source)
XLA Modules:
  0.0 373.7 jit_solution(15596140421105486915)
XLA Ops:
  13.3 83.1 %all-gather.2.cloned.1.call-done = bf16[8192,129]{0,1:T(8,128)(2,1)} async-done(((bf16[256,129]{0,1:T(8,128)(2,1)}), bf16[8192,129]{0,1:T(8,128)(2,1)}) %all-gather.2.cloned.1.call-update) | async-done | bytes 2113552 | tf_op jit(solution)/shard_map/all_gather | solution.py:17
  96.4 2.7 fusion.54
  105.9 35.0 %while.15 = (s32[]{:T(128)}, f32[256,1,2]{0,2,1:T(2,128)S(1)}, f32[256,1,2]{0,2,1:T(2,128)S(1)}, f32[256,1,2,64]{0,3,2,1:T(8,128)S(1)}, bf16[256]{0:T(256)(128)(...) while((s32[]{:T(128)}, f32[256,1,2]{0,2,1:T(2,128)S(1)}, ...), condition=%wide.region_5.6_spmd.clone, body=%wide.region_2.5_spmd.clone.sunk | while | flops 282692608 | bytes 32355992 | solution.py:158
  106.3 3.6 fusion.68
  110.0 3.5 fusion.71
  115.1 3.6 fusion.68
  118.7 3.5 fusion.71
  123.8 3.6 fusion.68
  127.5 3.5 fusion.71
  132.6 3.6 fusion.68
  136.2 3.5 fusion.71
  142.7 7.2 %all-to-all-start = ((bf16[16,128,256]{1,2,0:T(8,128)(2,1)}), bf16[16,128,256]{1,2,0:T(8,128)(2,1)S(1)}, u32[]{:S(2)}, u32[]{:S(2)}) async-start(bf16[16,128,256]{1,2,0:T(8,128)(2,1)} %bitcast.156), calls=%async_computation | async-start | bytes 2097152 | tf_op jit(solution)/shard_map/all_to_all | solution.py:32
  153.1 23.1 %all-to-all-done = bf16[16,128,256]{1,2,0:T(8,128)(2,1)S(1)} async-done(((bf16[16,128,256]{1,2,0:T(8,128)(2,1)}), bf16[16,128,256]{1,2,0:T(8,128)(2,1)S(1)}, u32[]{:S(2)}, u32[]{:S(2)}) %all-to-all-start) | async-done | bytes 1048608 | tf_op jit(solution)/shard_map/all_to_all | solution.py:32
  177.0 5.2 %all-to-all-start.1 = ((f32[16,1,256]{2,1,0:T(1,128)}), f32[16,1,256]{2,1,0:T(1,128)S(1)}, u32[]{:S(2)}, u32[]{:S(2)}) async-start(f32[16,1,256]{2,1,0:T(1,128)} %broadcast_in_dim.54), calls=%async_computation.1 | async-start | bytes 32768 | tf_op jit(solution)/shard_map/all_to_all | solution.py:38
  182.4 4.4 %all-to-all-done.1 = f32[16,1,256]{2,1,0:T(1,128)S(1)} async-done(((f32[16,1,256]{2,1,0:T(1,128)}), f32[16,1,256]{2,1,0:T(1,128)S(1)}, u32[]{:S(2)}, u32[]{:S(2)}) %all-to-all-start.1) | async-done | bytes 16416 | tf_op jit(solution)/shard_map/all_to_all | solution.py:38
  186.9 2.0 gather_fusion
  189.1 19.4 %all_to_all.31 = bf16[32,20,128]{2,1,0:T(8,128)(2,1)S(1)} all-to-all(bf16[32,20,128]{2,1,0:T(8,128)(2,1)S(1)} %broadcast_select_fusion.1), channel_id=1, replica_groups=mesh['sp'=32,'tp'=16] {'sp'}, dimensions={0} | all-to-all | bytes 327680 | tf_op jit(solution)/shard_map/all_to_all | solution.py:201
  209.1 65.6 %all_to_all.32 = bf16[16,640,128]{1,2,0:T(8,128)(2,1)S(1)} all-to-all(bf16[16,640,128]{1,2,0:T(8,128)(2,1)S(1)} %stack.17), channel_id=1, replica_groups=mesh['sp'=32,'tp'=16] {'tp'}, dimensions={0} | all-to-all | bytes 5242880 | tf_op jit(solution)/shard_map/all_to_all | solution.py:205
  277.8 2.2 copy.131
  280.0 5.3 %all-to-all-start.4 = ((bf16[16,32,20,128]{3,1,2,0:T(8,128)(2,1)}), bf16[16,32,20,128]{3,1,2,0:T(8,128)(2,1)}, u32[]{:S(2)}, u32[]{:S(2)}) async-start(bf16[16,32,20,128]{3,1,2,0:T(8,128)(2,1)} %bitcast.179), calls=%async_computation.4 | async-start | bytes 5242880 | tf_op jit(solution)/shard_map/all_to_all | solution.py:32
  285.8 59.6 %all-to-all-done.4 = bf16[16,32,20,128]{3,1,2,0:T(8,128)(2,1)} async-done(((bf16[16,32,20,128]{3,1,2,0:T(8,128)(2,1)}), bf16[16,32,20,128]{3,1,2,0:T(8,128)(2,1)}, u32[]{:S(2)}, u32[]{:S(2)}) %all-to-all-start.4) | async-done | bytes 2621472 | tf_op jit(solution)/shard_map/all_to_all | solution.py:32
  345.4 2.1 reduce_sum.107
  348.2 3.9 %all-to-all-start.5 = ((bf16[32,20,128]{2,1,0:T(8,128)(2,1)}), bf16[32,20,128]{2,1,0:T(8,128)(2,1)S(1)}, u32[]{:S(2)}, u32[]{:S(2)}) async-start(bf16[32,20,128]{2,1,0:T(8,128)(2,1)} %copy.112), calls=%async_computation.5 | async-start | bytes 393216 | tf_op jit(solution)/shard_map/all_to_all | solution.py:214
  352.1 12.3 %all-to-all-done.5 = bf16[32,20,128]{2,1,0:T(8,128)(2,1)S(1)} async-done(((bf16[32,20,128]{2,1,0:T(8,128)(2,1)}), bf16[32,20,128]{2,1,0:T(8,128)(2,1)S(1)}, u32[]{:S(2)}, u32[]{:S(2)}) %all-to-all-start.5) | async-done | bytes 163872 | tf_op jit(solution)/shard_map/all_to_all | solution.py:214
  (131 shorter events, 33.1 us)
Async XLA Ops:
  6.5 270.4 %copy-start = (bf16[1,256,2048]{2,1,0:T(8,128)(2,1)S(1)}, bf16[1,256,2048]{2,1,0:T(8,128)(2,1)}, u32[]{:S(2)}) copy-start(bf16[1,256,2048]{2,1,0:T(8,128)(2,1)} %param.29) | copy-start | bytes 3145732
  6.5 89.9 %all-gather.2.cloned.1.call-start = ((), (), s32[]{:S(2)}) async-start(), calls=%async_computation.6 | async-start | bytes 2297856 | tf_op jit(solution)/shard_map/all_gather | solution.py:17
  105.9 35.1 %copy-start.3 = (bf16[128,2048]{1,0:T(8,128)(2,1)S(1)}, bf16[128,2048]{1,0:T(8,128)(2,1)}, u32[]{:S(2)}) copy-start(bf16[128,2048]{1,0:T(8,128)(2,1)} %param.22) | copy-start | bytes 1572868
  110.0 3.5 copy-start.1
  118.7 3.5 copy-start.1
  127.5 3.5 copy-start.1
  136.2 3.5 copy-start.1
  140.9 9.0 %copy-start.4 = (s32[256,2]{0,1:T(2,128)S(1)}, s32[256,2]{0,1:T(2,128)}, u32[]{:S(2)}) copy-start(s32[256,2]{0,1:T(2,128)} %param.25) | copy-start | bytes 6148
  140.9 35.4 %copy-start.2 = (bf16[256,128]{1,0:T(8,128)(2,1)S(1)}, bf16[256,128]{1,0:T(8,128)(2,1)}, u32[]{:S(2)}) copy-start(bf16[256,128]{1,0:T(8,128)(2,1)} %param.23) | copy-start | bytes 196612
  140.9 45.9 %copy-start.6 = (f32[128]{0:T(128)S(1)}, f32[128]{0:T(128)}, u32[]{:S(2)}) copy-start(f32[128]{0:T(128)} %param.24) | copy-start | bytes 1540
  142.7 33.5 %all-to-all-start = ((bf16[16,128,256]{1,2,0:T(8,128)(2,1)}), bf16[16,128,256]{1,2,0:T(8,128)(2,1)S(1)}, u32[]{:S(2)}, u32[]{:S(2)}) async-start(bf16[16,128,256]{1,2,0:T(8,128)(2,1)} %bitcast.156), calls=%async_computation | async-start | bytes 2097152 | tf_op jit(solution)/shard_map/all_to_all | solution.py:32
  177.0 9.7 %all-to-all-start.1 = ((f32[16,1,256]{2,1,0:T(1,128)}), f32[16,1,256]{2,1,0:T(1,128)S(1)}, u32[]{:S(2)}, u32[]{:S(2)}) async-start(f32[16,1,256]{2,1,0:T(1,128)} %broadcast_in_dim.54), calls=%async_computation.1 | async-start | bytes 32768 | tf_op jit(solution)/shard_map/all_to_all | solution.py:38
  208.6 66.1 %copy-start.7 = (bf16[1,2048,256]{2,1,0:T(8,128)(2,1)S(1)}, bf16[1,2048,256]{2,1,0:T(8,128)(2,1)}, u32[]{:S(2)}) copy-start(bf16[1,2048,256]{2,1,0:T(8,128)(2,1)} %param.27) | copy-start | bytes 3145732
  274.7 1.2 copy-start.8
  277.8 7.8 %copy-start.5 = (f32[256,2]{0,1:T(2,128)S(1)}, f32[256,2]{0,1:T(2,128)}, u32[]{:S(2)}) copy-start(f32[256,2]{0,1:T(2,128)} %param.26) | copy-start | bytes 6148
  280.0 65.3 %all-to-all-start.4 = ((bf16[16,32,20,128]{3,1,2,0:T(8,128)(2,1)}), bf16[16,32,20,128]{3,1,2,0:T(8,128)(2,1)}, u32[]{:S(2)}, u32[]{:S(2)}) async-start(bf16[16,32,20,128]{3,1,2,0:T(8,128)(2,1)} %bitcast.179), calls=%async_computation.4 | async-start | bytes 5242880 | tf_op jit(solution)/shard_map/all_to_all | solution.py:32
  348.2 16.2 %all-to-all-start.5 = ((bf16[32,20,128]{2,1,0:T(8,128)(2,1)}), bf16[32,20,128]{2,1,0:T(8,128)(2,1)S(1)}, u32[]{:S(2)}, u32[]{:S(2)}) async-start(bf16[32,20,128]{2,1,0:T(8,128)(2,1)} %copy.112), calls=%async_computation.5 | async-start | bytes 393216 | tf_op jit(solution)/shard_map/all_to_all | solution.py:214
Sparse Core Ops, SparseCore 0:
  10.9 85.4 all-gather.1
